TPU v7x, 32 devices: a whole 2x2x4 slice. The times are simulated.
32 devices in a mesh: sp: 16 (over z, y, x), tp: 2 (over core).
Axes of the slice: x: 2, y: 2, z: 4, core: 2. Of those that a mesh axis runs over, the one named last changes fastest.
Arguments:
- activations: bfloat16 [2048, 2048], P('sp', 'tp'), may hold values from -200 to 200
- norm_gain: float32 [2048], replicated, may hold values from 0.1 to 1.9
- state_proj: bfloat16 [2048, 1024], P(None, 'tp'), may hold values from -0.125 to 0.125
- value_proj: bfloat16 [2048, 1024], P(None, 'tp'), may hold values from -0.125 to 0.125
- post_gate_proj: bfloat16 [2048, 1024], P(None, 'tp'), may hold values from -0.125 to 0.125
- pre_gate_proj: bfloat16 [2048, 1024], P(None, 'tp'), may hold values from -0.125 to 0.125
- input_map: bfloat16 [64, 16, 128], P('tp'), may hold values from -1.5 to 1.5
- output_map: float32 [64, 128, 16], P('tp'), may hold values from -0.5 to 0.5
- skip_gain: float32 [1024], P('tp'), may hold values from -4 to 4
- rotation: float32 [64, 64], P('tp'), may hold values from -3.140625 to 3.140625
- log_decay: float32 [2048, 64], P('sp', 'tp'), may hold values from -1.5 to 0, as said below
- initial_state: float32 [2, 64, 64], P(None, 'tp'), may hold values from -12 to 12
- conv_taps: bfloat16 [3, 1024], P(None, 'tp'), may hold values from -3.5 to 3.5
- state_out: bfloat16 [1024, 2048], P(None, 'tp'), may hold values from -0.125 to 0.125
- conv_out: bfloat16 [1024, 2048], P(None, 'tp'), may hold values from -0.125 to 0.125
Outputs:
- layer_out: bfloat16 [2048, 2048], P('sp', 'tp')
Inputs may be any that keep to these rules, and one draw needn't show every extreme that they name: `log_decay`: every entry is negative.
All inputs are finite; a program needn't handle non-finite values.
Results may differ from a plain program's by a relative error of at most 0.014.
Values may be sent and summed in bfloat16 or wider, within the bound.
A program may use at most 64 MiB of HBM per device.

v0:
```python
import math

import jax
import jax.numpy as jnp
from jax import lax
from jax.sharding import PartitionSpec as P

D = 2048
GROUP_CH = 16
STATE = 64
CONV_W = 3


EPS = 1e-06


def passed_along(block, axis, distance):
    devices = range(lax.axis_size(axis))
    route = [(i - distance, i) for i in devices if i - distance in devices]
    return lax.ppermute(block, axis, route)


def prefix(x, axis, combine, identity):
    count, place = (lax.axis_size(axis), lax.axis_index(axis))
    everything = jax.tree.map(lambda part: lax.all_gather(part, axis), x)
    start = jax.tree.map(
        lambda part, zero: jnp.broadcast_to(jnp.asarray(zero, part.dtype), part.shape), x, identity
    )

    def turn(k, before):
        reached = k < place
        new = combine(before, jax.tree.map(lambda part: part[k], everything))
        return jax.tree.map(lambda a, b: jnp.where(reached, a, b), new, before)

    return lax.fori_loop(0, count, turn, start)


def combine(earlier, later):
    early_are, early_aim, early_hre, early_him = earlier
    late_are, late_aim, late_hre, late_him = later
    return (
        early_are * late_are - early_aim * late_aim,
        early_are * late_aim + early_aim * late_are,
        late_are * early_hre - late_aim * early_him + late_hre,
        late_are * early_him + late_aim * early_hre + late_him,
    )


def on_device(
    activations,
    norm_gain,
    state_proj,
    value_proj,
    post_gate_proj,
    pre_gate_proj,
    input_map,
    output_map,
    skip_gain,
    rotation,
    log_decay,
    initial_state,
    conv_taps,
    state_out,
    conv_out,
):
    rows = activations.shape[0]
    weights_in = (state_proj, value_proj, post_gate_proj, pre_gate_proj)
    wide_piece = lax.all_gather(activations, "tp", axis=1, tiled=True).astype(jnp.float32)
    scaled_piece = (wide_piece * norm_gain[None, :]).astype(jnp.bfloat16)
    totals = tuple(
        (jnp.dot(scaled_piece, weight, preferred_element_type=jnp.float32) for weight in weights_in)
    )
    squares = jnp.sum(wide_piece * wide_piece, axis=1)
    scale = lax.rsqrt(squares / D + EPS)[:, None]
    drive_in, value, post_gate, pre_gate = [
        (total * scale).astype(jnp.bfloat16) for total in totals
    ]
    mixed_in = (pre_gate.astype(jnp.float32) * value.astype(jnp.float32)).astype(jnp.bfloat16)
    tail = passed_along(mixed_in[rows - (CONV_W - 1) :], "sp", 1)
    padded = jnp.concatenate([tail, mixed_in], axis=0)
    taps = conv_taps.astype(jnp.float32)
    conv = jnp.zeros(mixed_in.shape, jnp.float32)
    for k in range(CONV_W):
        conv = conv + padded[k : k + rows].astype(jnp.float32) * taps[k][None, :]
    hidden_conv = (post_gate.astype(jnp.float32) * conv).astype(jnp.bfloat16)
    groups = rotation.shape[0]
    states = groups * STATE
    grouped = drive_in.reshape(rows, groups, GROUP_CH)
    drive = jnp.einsum("tgc,gck->tgk", grouped, input_map, preferred_element_type=jnp.float32)
    drive = drive * jnp.sqrt(-jnp.expm1(2.0 * log_decay))[:, :, None]
    cum_log = jnp.cumsum(log_decay, axis=0)
    total_log = cum_log[rows - 1 :]
    back_mag = jnp.exp(total_log - cum_log)[:, :, None]
    lag = (rows - 1 - jnp.arange(rows, dtype=jnp.int32)).astype(jnp.float32)
    back_angle = rotation[None, :, :] * lag[:, None, None]
    back_cos = jnp.cos(back_angle)
    back_sin = jnp.sin(back_angle)
    drive_re = drive[:, :, :STATE]
    drive_im = drive[:, :, STATE:]
    end_re = jnp.sum(back_mag * (back_cos * drive_re - back_sin * drive_im), axis=0).reshape(
        1, states
    )
    end_im = jnp.sum(back_mag * (back_cos * drive_im + back_sin * drive_re), axis=0).reshape(
        1, states
    )
    whole_mag = jnp.exp(total_log)[:, :, None]
    whole_angle = rotation[None, :, :] * float(rows)
    whole_re = (whole_mag * jnp.cos(whole_angle)).reshape(1, states)
    whole_im = (whole_mag * jnp.sin(whole_angle)).reshape(1, states)
    zeros_row = jnp.zeros((1, states), jnp.float32)
    ones_row = jnp.ones((1, states), jnp.float32)
    prior = prefix(
        (whole_re, whole_im, end_re, end_im),
        "sp",
        combine,
        (ones_row, zeros_row, zeros_row, zeros_row),
    )
    prior_are, prior_aim, prior_hre, prior_him = prior
    init_re = initial_state[0].reshape(1, states)
    init_im = initial_state[1].reshape(1, states)
    enter_re = (prior_hre + prior_are * init_re - prior_aim * init_im).reshape(groups, STATE)
    enter_im = (prior_him + prior_are * init_im + prior_aim * init_re).reshape(groups, STATE)
    span = math.gcd(rows, 32)
    count = rows // span
    inner = jnp.arange(span, dtype=jnp.int32)
    inner_f = inner.astype(jnp.float32)
    lower = (inner[:, None] >= inner[None, :]).astype(jnp.float32)
    step_angle = rotation[None, :, :] * inner_f[:, None, None]
    step_cos = jnp.cos(step_angle)
    step_sin = jnp.sin(step_angle)
    next_angle = rotation[None, :, :] * (inner_f + 1.0)[:, None, None]
    next_cos = jnp.cos(next_angle)
    next_sin = jnp.sin(next_angle)

    def block_step(carry, pieces):
        h_re, h_im = carry
        decay_block, drive_block = pieces
        rel = jnp.cumsum(decay_block, axis=0)[:, :, None]
        down = jnp.exp(-rel)
        upward = jnp.exp(rel)
        d_re = drive_block[:, :, :STATE]
        d_im = drive_block[:, :, STATE:]
        u_re = down * (step_cos * d_re + step_sin * d_im)
        u_im = down * (step_cos * d_im - step_sin * d_re)
        s_re = jnp.einsum("ts,sgp->tgp", lower, u_re, precision=lax.Precision.HIGHEST)
        s_im = jnp.einsum("ts,sgp->tgp", lower, u_im, precision=lax.Precision.HIGHEST)
        state_re = upward * (
            step_cos * s_re - step_sin * s_im + next_cos * h_re[None] - next_sin * h_im[None]
        )
        state_im = upward * (
            step_cos * s_im + step_sin * s_re + next_cos * h_im[None] + next_sin * h_re[None]
        )
        stacked = jnp.concatenate([state_re, state_im], axis=2)
        read_block = jnp.einsum(
            "tgk,gkc->tgc", stacked, output_map, precision=lax.Precision.HIGHEST
        ).reshape(span, groups * GROUP_CH)
        return ((state_re[span - 1], state_im[span - 1]), read_block)

    ignored, reads = lax.scan(
        block_step,
        (enter_re, enter_im),
        (log_decay.reshape(count, span, groups), drive.reshape(count, span, groups, 2 * STATE)),
    )
    read = reads.reshape(rows, groups * GROUP_CH)
    hidden_state = jax.nn.gelu(read + skip_gain[None, :] * drive_in.astype(jnp.float32)).astype(
        jnp.bfloat16
    )
    pieces = (
        lax.all_gather(hidden_state, "tp", axis=1, tiled=True),
        lax.all_gather(hidden_conv, "tp", axis=1, tiled=True),
    )
    summed = jnp.dot(pieces[0], state_out, preferred_element_type=jnp.float32) + jnp.dot(
        pieces[1], conv_out, preferred_element_type=jnp.float32
    )
    return summed.astype(jnp.bfloat16)


def solution(mesh):
    return jax.shard_map(
        on_device,
        mesh=mesh,
        in_specs=(
            P("sp", "tp"),
            P(),
            P(None, "tp"),
            P(None, "tp"),
            P(None, "tp"),
            P(None, "tp"),
            P("tp", None, None),
            P("tp", None, None),
            P("tp"),
            P("tp", None),
            P("sp", "tp"),
            P(None, "tp", None),
            P(None, "tp"),
            P(None, "tp"),
            P(None, "tp"),
        ),
        out_specs=P("sp", "tp"),
        check_vma=False,
    )
```

profile of v0, /device:TPU:0, one launch (start us, length us, event | category | flops | bytes accessed | tf_op | source)
XLA Modules:
  0.0 258.8 jit_solution(2107934273433321480)
XLA Ops:
  0.0 2.6 %all_gather.23 = bf16[128,2048]{1,0:T(8,128)(2,1)S(1)} all-gather(bf16[128,1024]{1,0:T(8,128)(2,1)} %param.19), channel_id=1, replica_groups=mesh['sp'=16,'tp'=2] {'tp'}, dimensions={1}, use_global_device_ids=true | all-gather | bytes 786432 | tf_op jit(solution)/shard_map/all_gather | solution.py:68
  2.7 0.2 fusion.78
  2.9 2.1 fusion.76
  5.0 0.4 fusion.74
  5.4 0.6 slice.75
  6.0 5.3 %collective-permute-start = (bf16[2,512]{1,0:T(2,128)(2,1)}, bf16[2,512]{1,0:T(2,128)(2,1)}, u32[]{:S(2)}, u32[]{:S(2)}) collective-permute-start(bf16[2,512]{1,0:T(2,128)(2,1)} %slice.75), channel_id=1, source_target_pairs={{0,2},{2,4},{4,6},{6,8},{8,10},{10,12},{12,14},{14,16},{16,18},{18... | collective-permute-start | bytes 6152 | tf_op jit(solution)/shard_map/ppermute | solution.py:20
  11.4 0.1 copy.35
  11.5 0.5 broadcast_add_fusion
  12.1 0.6 iota_convert_fusion
  12.6 2.0 fusion.66
  14.7 0.1 copy.37
  14.8 0.2 reduce_window_sum.22
  15.1 1.8 bitcast_multiply_fusion.8
  16.9 3.1 %copy.39 = f32[128,32,128]{2,1,0:T(8,128)} copy(f32[128,32,128]{0,2,1:T(8,128)} %bitcast_multiply_fusion.8) | data formatting | bytes 4194304 | tf_op jit(solution)/shard_map/mul | solution.py:90
  20.0 7.3 %fusion.84 = (f32[32,64]{1,0:T(8,128)S(1)}, f32[32,64]{1,0:T(8,128)S(1)}) fusion(f32[128,32,128]{0,2,1:T(8,128)} %bitcast_multiply_fusion.8, f32[128]{0:T(128)S(1)} %subtract_convert_fusion, f32[32,64]{1,0:T(8,128)} %param.28, f32[128,32]{0,1:T(8,128)S(1)} %copy.36), kind=kLoop, calls=%fused_computation.117 | loop fusion | flops 2879488 | bytes 2138624 | tf_op jit(solution)/shard_map/reduce_sum | solution.py:103
  27.4 0.1 all_gather_reshape.14
  27.5 39.0 %all_gather.24 = f32[16,1,2048]{2,1,0:T(1,128)S(1)} all-gather(f32[1,1,2048]{2,1,0:T(1,128)S(1)} %all_gather_reshape.14), channel_id=1, replica_groups=mesh['sp'=16,'tp'=2] {'sp'}, dimensions={0}, use_global_device_ids=true | all-gather | bytes 139264 | tf_op jit(solution)/shard_map/all_gather | solution.py:25
  66.6 36.1 %all_gather.25 = f32[16,1,2048]{2,1,0:T(1,128)S(1)} all-gather(f32[1,1,2048]{2,1,0:T(1,128)S(1)} %all_gather_reshape.15), channel_id=1, replica_groups=mesh['sp'=16,'tp'=2] {'sp'}, dimensions={0}, use_global_device_ids=true | all-gather | bytes 139264 | tf_op jit(solution)/shard_map/all_gather | solution.py:25
  102.7 0.8 sine_multiply_fusion
  103.5 0.1 all_gather_reshape.12
  103.6 38.1 %all_gather.21 = f32[16,1,2048]{2,1,0:T(1,128)S(1)} all-gather(f32[1,1,2048]{2,1,0:T(1,128)S(1)} %all_gather_reshape.12), channel_id=1, replica_groups=mesh['sp'=16,'tp'=2] {'sp'}, dimensions={0}, use_global_device_ids=true | all-gather | bytes 139264 | tf_op jit(solution)/shard_map/all_gather | solution.py:25
  141.7 0.1 all_gather_reshape.13
  141.8 36.1 %all_gather.22 = f32[16,1,2048]{2,1,0:T(1,128)S(1)} all-gather(f32[1,1,2048]{2,1,0:T(1,128)S(1)} %all_gather_reshape.13), channel_id=1, replica_groups=mesh['sp'=16,'tp'=2] {'sp'}, dimensions={0}, use_global_device_ids=true | all-gather | bytes 139264 | tf_op jit(solution)/shard_map/all_gather | solution.py:25
  177.9 1.4 while.37
  179.4 0.1 reshape_squeeze.6
  179.7 70.8 %while.38 = (s32[]{:T(128)}, f32[32,64]{1,0:T(8,128)S(1)}, f32[32,64]{1,0:T(8,128)S(1)}, f32[4,32,512]{2,1,0:T(8,128)}, f32[4,32,32]{2,1,0:T(8,128)S(1)}, /*inde...) while((s32[]{:T(128)}, f32[32,64]{1,0:T(8,128)S(1)}, ...), condition=%wide.region_8.9_spmd.clone.clone.clone, body=%wide.region_6.8_spmd.clone.clone.clone.sunk | while | flops 77500416 | bytes 8878365 | solution.py:159
  179.9 1.1 constant_dynamic-slice_fusion.4
  181.0 0.3 copy.55
  181.3 0.8 copy-done.3
  182.1 4.6 %convolution_bitcast_fusion.3 = f32[32,32,64]{2,0,1:T(8,128)} fusion(f32[32,32,128]{2,0,1:T(8,128)S(1)} %bitcast.115, f32[32]{0:T(128)} %get-tuple-element.680, f32[32,64]{1,0:T(8,128)} %get-tuple-element.681, f32[32,32]{0,1:T(8,128)S(1)} %copy.56), kind=kOutput, calls=%fused_computation.29.clone.1 | convolution fusion | flops 25495552 | bytes 1335424 | tf_op jit(solution)/shard_map/while/body/eval_jaxpr/ts,sgp->tgp/dot_general | solution.py:146
  186.8 7.9 %fusion.125 = (f32[32,32,64]{2,0,1:T(8,128)S(1)}, f32[32,32,64]{2,0,1:T(8,128)S(1)}) fusion(f32[32,32,64]{2,0,1:T(8,128)} %convolution_bitcast_fusion.3, f32[32]{0:T(128)} %get-tuple-element.682, f32[32]{0:T(128)} %get-tuple-element.680, f32[32,64]{1,0:T(8,128)} %get-tuple-element.681, f32[32,64]{1,0:T(8,128)S(1)} %get-tuple-element.663, ...), kind=kOutput, calls=%fused_computation.50.clone.1 | convolution fusion | flops 26675200 | bytes 2156032 | tf_op jit(solution)/shard_map/while/body/eval_jaxpr/ts,sgp->tgp/dot_general | solution.py:145
  194.6 2.0 fusion.126
  196.6 0.1 copy.58
  196.7 0.6 constant_dynamic-update-slice_fusion.2
  197.6 1.1 constant_dynamic-slice_fusion.4
  198.7 0.3 copy.55
  199.0 0.8 copy-done.3
  199.8 4.6 %convolution_bitcast_fusion.3 = f32[32,32,64]{2,0,1:T(8,128)} fusion(f32[32,32,128]{2,0,1:T(8,128)S(1)} %bitcast.115, f32[32]{0:T(128)} %get-tuple-element.680, f32[32,64]{1,0:T(8,128)} %get-tuple-element.681, f32[32,32]{0,1:T(8,128)S(1)} %copy.56), kind=kOutput, calls=%fused_computation.29.clone.1 | convolution fusion | flops 25495552 | bytes 1335424 | tf_op jit(solution)/shard_map/while/body/eval_jaxpr/ts,sgp->tgp/dot_general | solution.py:146
  204.5 7.9 %fusion.125 = (f32[32,32,64]{2,0,1:T(8,128)S(1)}, f32[32,32,64]{2,0,1:T(8,128)S(1)}) fusion(f32[32,32,64]{2,0,1:T(8,128)} %convolution_bitcast_fusion.3, f32[32]{0:T(128)} %get-tuple-element.682, f32[32]{0:T(128)} %get-tuple-element.680, f32[32,64]{1,0:T(8,128)} %get-tuple-element.681, f32[32,64]{1,0:T(8,128)S(1)} %get-tuple-element.663, ...), kind=kOutput, calls=%fused_computation.50.clone.1 | convolution fusion | flops 26675200 | bytes 2156032 | tf_op jit(solution)/shard_map/while/body/eval_jaxpr/ts,sgp->tgp/dot_general | solution.py:145
  212.4 2.0 fusion.126
  214.3 0.1 copy.58
  214.4 0.6 constant_dynamic-update-slice_fusion.2
  215.3 1.1 constant_dynamic-slice_fusion.4
  216.4 0.3 copy.55
  216.7 0.8 copy-done.3
  217.5 4.6 %convolution_bitcast_fusion.3 = f32[32,32,64]{2,0,1:T(8,128)} fusion(f32[32,32,128]{2,0,1:T(8,128)S(1)} %bitcast.115, f32[32]{0:T(128)} %get-tuple-element.680, f32[32,64]{1,0:T(8,128)} %get-tuple-element.681, f32[32,32]{0,1:T(8,128)S(1)} %copy.56), kind=kOutput, calls=%fused_computation.29.clone.1 | convolution fusion | flops 25495552 | bytes 1335424 | tf_op jit(solution)/shard_map/while/body/eval_jaxpr/ts,sgp->tgp/dot_general | solution.py:146
  222.2 7.9 %fusion.125 = (f32[32,32,64]{2,0,1:T(8,128)S(1)}, f32[32,32,64]{2,0,1:T(8,128)S(1)}) fusion(f32[32,32,64]{2,0,1:T(8,128)} %convolution_bitcast_fusion.3, f32[32]{0:T(128)} %get-tuple-element.682, f32[32]{0:T(128)} %get-tuple-element.680, f32[32,64]{1,0:T(8,128)} %get-tuple-element.681, f32[32,64]{1,0:T(8,128)S(1)} %get-tuple-element.663, ...), kind=kOutput, calls=%fused_computation.50.clone.1 | convolution fusion | flops 26675200 | bytes 2156032 | tf_op jit(solution)/shard_map/while/body/eval_jaxpr/ts,sgp->tgp/dot_general | solution.py:145
  230.1 2.0 fusion.126
  232.0 0.1 copy.58
  232.1 0.6 constant_dynamic-update-slice_fusion.2
  233.0 1.1 constant_dynamic-slice_fusion.4
  234.1 0.3 copy.55
  234.4 0.8 copy-done.3
  235.2 4.6 %convolution_bitcast_fusion.3 = f32[32,32,64]{2,0,1:T(8,128)} fusion(f32[32,32,128]{2,0,1:T(8,128)S(1)} %bitcast.115, f32[32]{0:T(128)} %get-tuple-element.680, f32[32,64]{1,0:T(8,128)} %get-tuple-element.681, f32[32,32]{0,1:T(8,128)S(1)} %copy.56), kind=kOutput, calls=%fused_computation.29.clone.1 | convolution fusion | flops 25495552 | bytes 1335424 | tf_op jit(solution)/shard_map/while/body/eval_jaxpr/ts,sgp->tgp/dot_general | solution.py:146
  239.9 7.9 %fusion.125 = (f32[32,32,64]{2,0,1:T(8,128)S(1)}, f32[32,32,64]{2,0,1:T(8,128)S(1)}) fusion(f32[32,32,64]{2,0,1:T(8,128)} %convolution_bitcast_fusion.3, f32[32]{0:T(128)} %get-tuple-element.682, f32[32]{0:T(128)} %get-tuple-element.680, f32[32,64]{1,0:T(8,128)} %get-tuple-element.681, f32[32,64]{1,0:T(8,128)S(1)} %get-tuple-element.663, ...), kind=kOutput, calls=%fused_computation.50.clone.1 | convolution fusion | flops 26675200 | bytes 2156032 | tf_op jit(solution)/shard_map/while/body/eval_jaxpr/ts,sgp->tgp/dot_general | solution.py:145
  247.8 2.0 fusion.126
  249.7 0.1 copy.58
  249.8 0.6 constant_dynamic-update-slice_fusion.2
  250.6 1.3 fusion.96
  251.9 2.0 all_gather.26
  253.8 0.4 fusion.101
  254.4 1.3 fusion.70
  255.7 2.0 all_gather.27
  257.7 1.2 fusion.65
  (97 shorter events, 2.7 us)
Async XLA Ops:
  0.0 253.8 %copy-start = (bf16[1024,1024]{1,0:T(8,128)(2,1)S(1)}, bf16[1024,1024]{1,0:T(8,128)(2,1)}, u32[]{:S(2)}) copy-start(bf16[1024,1024]{1,0:T(8,128)(2,1)} %param.32) | copy-start | bytes 6291460
  0.0 4.9 %copy-start.10 = (f32[2048]{0:T(1024)S(1)}, f32[2048]{0:T(1024)}, u32[]{:S(2)}) copy-start(f32[2048]{0:T(1024)} %param.20) | copy-start | bytes 24580
  0.0 4.9 %copy-start.4 = (bf16[2048,512]{1,0:T(8,128)(2,1)S(1)}, bf16[2048,512]{1,0:T(8,128)(2,1)}, u32[]{:S(2)}) copy-start(bf16[2048,512]{1,0:T(8,128)(2,1)} %param.24) | copy-start | bytes 6291460
  2.7 10.0 %copy-start.1 = (bf16[128,2048]{1,0:T(8,128)(2,1)}, bf16[128,2048]{1,0:T(8,128)(2,1)S(1)}, u32[]{:S(2)}) copy-start(bf16[128,2048]{1,0:T(8,128)(2,1)S(1)} %all_gather.23) | copy-start | bytes 1572868
  4.9 6.4 %copy-start.11 = (f32[128,32]{0,1:T(8,128)S(1)}, f32[128,32]{0,1:T(8,128)}, u32[]{:S(2)}) copy-start(f32[128,32]{0,1:T(8,128)} %param.29) | copy-start | bytes 49156
  5.4 5.9 %copy-start.7 = (bf16[128,512]{1,0:T(8,128)(2,1)}, bf16[128,512]{1,0:T(8,128)(2,1)S(1)}, u32[]{:S(2)}) copy-start(bf16[128,512]{1,0:T(8,128)(2,1)S(1)} %fusion.74) | copy-start | bytes 393220
  5.4 9.7 %copy-start.9 = (bf16[32,16,128]{2,1,0:T(8,128)(2,1)S(1)}, bf16[32,16,128]{2,1,0:T(8,128)(2,1)}, u32[]{:S(2)}) copy-start(bf16[32,16,128]{2,1,0:T(8,128)(2,1)} %param.25) | copy-start | bytes 393220
  6.0 248.3 %collective-permute-start = (bf16[2,512]{1,0:T(2,128)(2,1)}, bf16[2,512]{1,0:T(2,128)(2,1)}, u32[]{:S(2)}, u32[]{:S(2)}) collective-permute-start(bf16[2,512]{1,0:T(2,128)(2,1)} %slice.75), channel_id=1, source_target_pairs={{0,2},{2,4},{4,6},{6,8},{8,10},{10,12},{12,14},{14,16},{16,18},{18... | collective-permute-start | bytes 6152 | tf_op jit(solution)/shard_map/ppermute | solution.py:20
  14.7 5.4 %copy-start.6 = (bf16[128,512]{1,0:T(8,128)(2,1)}, bf16[128,512]{1,0:T(8,128)(2,1)S(1)}, u32[]{:S(2)}) copy-start(bf16[128,512]{1,0:T(8,128)(2,1)S(1)} %fusion.66) | copy-start | bytes 393220
  20.0 159.3 %copy-start.12 = (f32[2,32,64]{2,1,0:T(8,128)S(1)}, f32[2,32,64]{2,1,0:T(8,128)}, u32[]{:S(2)}) copy-start(f32[2,32,64]{2,1,0:T(8,128)} %param.30) | copy-start | bytes 49156
  179.7 70.9 %copy-start.14 = (f32[512]{0:T(512)S(1)}, f32[512]{0:T(512)}, u32[]{:S(2)}) copy-start(f32[512]{0:T(512)} %param.27) | copy-start | bytes 6148
  181.3 0.8 copy-start.3
  199.0 0.8 copy-start.3
  216.7 0.8 copy-start.3
  234.4 0.8 copy-start.3
  250.5 3.8 %copy-start.13 = (bf16[3,512]{1,0:T(4,128)(2,1)S(1)}, bf16[3,512]{1,0:T(4,128)(2,1)}, u32[]{:S(2)}) copy-start(bf16[3,512]{1,0:T(4,128)(2,1)} %param.31) | copy-start | bytes 9220
  250.6 3.8 %copy-start.2 = (bf16[128,2048]{1,0:T(8,128)(2,1)S(1)}, bf16[128,2048]{1,0:T(8,128)(2,1)}, u32[]{:S(2)}) copy-start(bf16[128,2048]{1,0:T(8,128)(2,1)} %copy-done.1) | copy-start | bytes 1572868
  250.6 3.8 %copy-start.8 = (bf16[128,512]{1,0:T(8,128)(2,1)S(1)}, bf16[128,512]{1,0:T(8,128)(2,1)}, u32[]{:S(2)}) copy-start(bf16[128,512]{1,0:T(8,128)(2,1)} %copy-done.7) | copy-start | bytes 393220
  250.6 3.8 %copy-start.15 = (bf16[2048,512]{1,0:T(8,128)(2,1)S(1)}, bf16[2048,512]{1,0:T(8,128)(2,1)}, u32[]{:S(2)}) copy-start(bf16[2048,512]{1,0:T(8,128)(2,1)} %param.23) | copy-start | bytes 6291460
  254.3 3.3 %copy-start.5 = (bf16[1024,1024]{1,0:T(8,128)(2,1)S(1)}, bf16[1024,1024]{1,0:T(8,128)(2,1)}, u32[]{:S(2)}) copy-start(bf16[1024,1024]{1,0:T(8,128)(2,1)} %param.33) | copy-start | bytes 6291460
where the time goes:
time: 260 us; the launch traced here: 259 us
  blocking collectives  156 us (60%)
  matrix products  67 us (26%)
  local copies, waits for them, and re-layouts  17.2 us (7%)
  other arithmetic  12.3 us (5%)
  starting transfers between devices  5.31 us (2%)
    all_gather x4, blocking collectives, prefix(): everything = jax.tree.map(lambda part: lax.all_gather(part, axis), x)  149 us
    dot_general x4, matrix products, block_step(): jnp.einsum('ts,sgp->tgp', lower, u_re, precision=lax.Precision.HIGHEST)  31.5 us
    dot_general x4, matrix products, block_step(): jnp.einsum('ts,sgp->tgp', lower, u_im, precision=lax.Precision.HIGHEST)  18.5 us
    dot_general x4, matrix products, block_step(): jnp.einsum('tgk,gkc->tgc', stacked, output_map, precision=lax.Precision.H...  7.84 us
    reduce_sum x1, other arithmetic, on_device(): jnp.sum(back_mag * (back_cos * drive_im + back_sin * drive_re), axis=0)  7.34 us
    dot_general x4, matrix products, on_device(): jnp.dot(scaled_piece, weight, preferred_element_type=jnp.float32)  5.82 us
    dynamic_slice x8, local copies, waits for them, and re-layouts, on_device(): lax.scan(block_step, (enter_re, enter_im), (log_decay.reshape(count, span...  5.56 us
    ppermute x1, starting transfers between devices, passed_along(): return lax.ppermute(block, axis, route)  5.31 us
  transfers between devices with their start and end apart: 1, of which 0 were waited for; matrix products, arithmetic and copies ran while one was open for 34% of the time, Pallas kernels for 0%

commit v1 on v0

v1 whole, which is shorter than its diff:
```python
import functools

import jax
import jax.numpy as jnp
from jax import lax
from jax.experimental import pallas as pl
from jax.experimental.pallas import tpu as pltpu
from jax.sharding import PartitionSpec as P

EPS = 1e-06
LANES = 128
MESH = pl.DeviceIdType.MESH
F32 = jnp.float32
BF16 = jnp.bfloat16


def minus_expm1(y):
    poly = jnp.ones_like(y)
    for k in range(11, 1, -1):
        poly = 1.0 + poly * y * (1.0 / k)
    return jnp.where(y > -0.5, -y * poly, 1.0 - jnp.exp(y))


def split3(v):
    hi = v.astype(BF16)
    rest = v - hi.astype(F32)
    mid = rest.astype(BF16)
    low = (rest - mid.astype(F32)).astype(BF16)
    return hi, mid, low


def cmul(a, b):
    return a[0] * b[0] - a[1] * b[1], a[0] * b[1] + a[1] * b[0]


def cpow(base, count):
    result = None
    while count:
        if count & 1:
            result = base if result is None else cmul(result, base)
        count >>= 1
        if count:
            base = cmul(base, base)
    return result


def gelu(x):
    return 0.5 * x * (1.0 + jnp.tanh(0.7978845608028654 * (x + 0.044715 * x * x * x)))


def kernel(
    n,
    x_ref,
    gain_ref,
    w0_hbm,
    w1_hbm,
    w2_hbm,
    w3_hbm,
    imap_ref,
    omap_ref,
    skip_ref,
    rot_ref,
    ld_ref,
    init_ref,
    taps_ref,
    so_hbm,
    co_hbm,
    out_ref,
    wv,
    ov,
    xr,
    acc,
    din,
    bd_in,
    bd_out,
    wide_w,
    mag,
    drv,
    pairs,
    pad,
    pay,
    ends,
    hs,
    hc,
    oacc,
    wsem,
    osem,
    x_sem,
    tail_sem,
    hc_sem,
    hs_sem,
    send_sem,
    recv_sem,
):
    sp, tp = lax.axis_index("sp"), lax.axis_index("tp")
    other = 1 - tp
    rows, half = x_ref.shape
    groups, state = rot_ref.shape
    gch = imap_ref.shape[1]
    chans = groups * gch
    states = groups * state
    prow = states // LANES
    per_block = LANES // gch
    blocks = groups // per_block
    quads = prow // blocks
    bstates = quads * LANES
    cwide = taps_ref.shape[1]
    width = taps_ref.shape[0]

    barrier = pltpu.get_barrier_semaphore()

    def greet(j, c):
        pl.semaphore_signal(
            barrier, inc=1, device_id={"sp": lax.rem(sp + j, n), "tp": tp}, device_id_type=MESH
        )
        return c

    pl.semaphore_signal(barrier, inc=1, device_id={"sp": sp, "tp": other}, device_id_type=MESH)
    lax.fori_loop(1, n, greet, 0)

    wcopies = {}
    for h, part in ((0, tp), (1, other)):
        for i, w in enumerate((w0_hbm, w1_hbm, w2_hbm, w3_hbm)):
            copy = pltpu.make_async_copy(
                w.at[pl.ds(part * half, half), :], wv.at[i, h], wsem.at[i, h]
            )
            copy.start()
            wcopies[i, h] = copy
    ocopies = {}
    for i, w, deep in ((1, co_hbm, cwide), (0, so_hbm, chans)):
        for h, part in ((0, tp), (1, other)):
            copy = pltpu.make_async_copy(w.at[pl.ds(part * deep, deep), :], ov.at[i, h], osem.at[i, h])
            copy.start()
            ocopies[i, h] = copy

    lane = lax.broadcasted_iota(jnp.int32, (1, LANES), 1)
    for i, v in enumerate((rot_ref[...], init_ref[0], init_ref[1])):
        pairs[pl.ds(i * groups, groups), :] = jnp.concatenate([v, v], axis=1)

    def paired(i):
        even = pairs[pl.ds(i * groups, prow, stride=2), :]
        odd = pairs[pl.ds(i * groups + 1, prow, stride=2), :]
        return jnp.where(lane < state, even, odd)

    theta = paired(0)
    cosv, sinv = jnp.cos(theta), jnp.sin(theta)
    whole = cpow((cosv, sinv), rows)

    for src, dst in ((imap_ref, bd_in), (omap_ref, bd_out)):
        dst[...] = jnp.zeros_like(dst)
        for b in range(blocks):
            for q in range(quads):
                g = b * per_block + 2 * q
                one = src[g].astype(F32)
                two = src[g + 1].astype(F32)
                one_r = jnp.concatenate([one[:, state:], one[:, :state]], axis=1)
                two_r = jnp.concatenate([two[:, state:], two[:, :state]], axis=1)
                low = lane < state
                re = jnp.concatenate([jnp.where(low, one, 0.0), jnp.where(low, 0.0, two_r)], axis=0)
                im = jnp.concatenate([jnp.where(low, one_r, 0.0), jnp.where(low, 0.0, two)], axis=0)
                at = pl.ds(b * LANES + q * 2 * gch, 2 * gch)
                dst[at, q * LANES : (q + 1) * LANES] = re.astype(BF16)
                dst[at, bstates + q * LANES : bstates + (q + 1) * LANES] = im.astype(BF16)

    ld = ld_ref[...].T
    mags = split3(jnp.exp(ld))
    gains = split3(jnp.sqrt(minus_expm1(2.0 * ld)))[:2]
    for b in range(blocks):
        col = lax.broadcasted_iota(jnp.int32, (groups, bstates), 1) + b * bstates
        row = lax.broadcasted_iota(jnp.int32, (groups, bstates), 0)
        spread = jnp.where(
            (col >= row * state) & (col < (row + 1) * state), 1.0, 0.0
        ).astype(BF16)

        def over(pieces):
            total = None
            for piece in pieces:
                d = jnp.dot(piece, spread, preferred_element_type=F32)
                total = d if total is None else total + d
            return total

        m = over(mags)
        for q in range(quads):
            mag[pl.ds(b * quads + q, rows, stride=prow), :] = m[:, q * LANES : (q + 1) * LANES]
        wide_w[:, b * bstates : (b + 1) * bstates] = over(gains)

    pl.semaphore_wait(barrier, n)
    partner = {"sp": sp, "tp": other}

    def remote(src, dst, s, r, dev):
        return pltpu.make_async_remote_copy(
            src_ref=src, dst_ref=dst, send_sem=s, recv_sem=r, device_id=dev, device_id_type=MESH
        )

    x_copy = remote(x_ref, xr, x_sem.at[0], x_sem.at[1], partner)
    x_copy.start()

    own = x_ref[...].astype(F32)
    scaled = (own * gain_ref[:, pl.ds(pl.multiple_of(tp * half, LANES), half)]).astype(BF16)
    squares = jnp.sum(own * own, axis=1, keepdims=True)
    for i in range(4):
        wcopies[i, 0].wait()
        acc[i] = jnp.dot(scaled, wv[i, 0], preferred_element_type=F32)

    x_copy.wait_recv()
    far = xr[...].astype(F32)
    scaled_far = (far * gain_ref[:, pl.ds(pl.multiple_of(other * half, LANES), half)]).astype(BF16)
    squares = squares + jnp.sum(far * far, axis=1, keepdims=True)
    scale = lax.rsqrt(squares / (2 * half) + EPS)

    def project(i):
        wcopies[i, 1].wait()
        total = acc[i] + jnp.dot(scaled_far, wv[i, 1], preferred_element_type=F32)
        return (total * scale).astype(BF16)

    drive_in = project(0)
    din[...] = drive_in
    for b in range(blocks):
        blk = jnp.dot(
            drive_in[:, b * LANES : (b + 1) * LANES],
            bd_in[b * LANES : (b + 1) * LANES, :],
            preferred_element_type=F32,
        )
        for q in range(quads):
            r = b * quads + q
            w = wide_w[:, r * LANES : (r + 1) * LANES]
            drv[pl.ds(r, rows, stride=2 * prow), :] = blk[:, q * LANES : (q + 1) * LANES] * w
            drv[pl.ds(prow + r, rows, stride=2 * prow), :] = (
                blk[:, bstates + q * LANES : bstates + (q + 1) * LANES] * w
            )

    def advance(t, h):
        m = mag[pl.ds(pl.multiple_of(t * prow, prow), prow), :]
        base = pl.multiple_of(t * 2 * prow, 2 * prow)
        d_re = drv[pl.ds(base, prow), :]
        d_im = drv[pl.ds(base + prow, prow), :]
        f_re, f_im = m * cosv, m * sinv
        new_re = (f_re * h[0] + d_re) - f_im * h[1]
        new_im = (f_re * h[1] + d_im) + f_im * h[0]
        return m, base, (new_re, new_im)

    def first(t, c):
        m, base, h = advance(t, c[:2])
        return h[0], h[1], c[2] * m

    zero = jnp.zeros((prow, LANES), F32)
    e_re, e_im, e_mag = lax.fori_loop(0, rows, first, (zero, zero, zero + 1.0), unroll=8)
    pay[pl.ds(0, prow), :] = e_re
    pay[pl.ds(prow, prow), :] = e_im
    pay[pl.ds(2 * prow, prow), :] = e_mag

    def end_copy(j):
        return remote(
            pay, ends.at[sp], send_sem.at[j], recv_sem.at[sp], {"sp": j, "tp": tp}
        )

    def send_end(j, c):
        end_copy(j).start()
        return c

    lax.fori_loop(sp + 1, n, send_end, 0)

    value = project(1)
    pre_gate = project(3)
    mixed = (pre_gate.astype(F32) * value.astype(F32)).astype(BF16).astype(F32)
    pad[pl.ds(8, rows), :] = mixed
    tail_copy = remote(
        pad.at[pl.ds(rows, 8), :],
        pad.at[pl.ds(0, 8), :],
        tail_sem.at[0],
        tail_sem.at[1],
        {"sp": lax.rem(sp + 1, n), "tp": tp},
    )

    @pl.when(sp < n - 1)
    def _():
        tail_copy.start()

    post_gate = project(2).astype(F32)

    @pl.when(sp == 0)
    def _():
        pad[pl.ds(0, 8), :] = jnp.zeros((8, cwide), F32)

    @pl.when(sp > 0)
    def _():
        tail_copy.wait_recv()

    conv = jnp.zeros((rows, cwide), F32)
    for k in range(width):
        conv = conv + pad[pl.ds(8 + k - (width - 1), rows), :] * taps_ref[k : k + 1, :].astype(F32)
    hc[0] = (post_gate * conv).astype(BF16)
    hc_copy = remote(hc.at[0], hc.at[1], hc_sem.at[0], hc_sem.at[1], partner)
    hc_copy.start()
    ocopies[1, 0].wait()
    ocopies[1, 1].wait()
    oacc[...] = jnp.dot(hc[0], ov[1, 0], preferred_element_type=F32)
    hc_copy.wait_recv()
    oacc[...] += jnp.dot(hc[1], ov[1, 1], preferred_element_type=F32)

    def gather(k, h):
        remote(pay, ends.at[k], send_sem.at[k], recv_sem.at[k], {"sp": k, "tp": tp}).wait_recv()
        k_mag = ends[k, pl.ds(2 * prow, prow), :]
        moved = cmul((whole[0] * k_mag, whole[1] * k_mag), h)
        return moved[0] + ends[k, pl.ds(0, prow), :], moved[1] + ends[k, pl.ds(prow, prow), :]

    enter = lax.fori_loop(0, sp, gather, (paired(1), paired(2)))

    def second(t, c):
        m, base, h = advance(t, c)
        drv[pl.ds(base, prow), :] = h[0]
        drv[pl.ds(base + prow, prow), :] = h[1]
        return h

    lax.fori_loop(0, rows, second, enter, unroll=8)

    hs_copies = []
    for b in range(blocks):
        at = [b * quads + q for q in range(quads)]
        at = at + [prow + r for r in at]
        cols = slice(b * LANES, (b + 1) * LANES)
        st = jnp.concatenate(
            [drv[pl.ds(r, rows, stride=2 * prow), :].astype(BF16) for r in at], axis=1
        )
        read = lax.dot_general(
            st, bd_out[cols, :], (((1,), (1,)), ((), ())), preferred_element_type=F32
        )
        hs[0, :, cols] = gelu(read + skip_ref[:, cols] * din[:, cols].astype(F32)).astype(BF16)
        if b % 2 == 1:
            two = pl.ds((b - 1) * LANES, 2 * LANES)
            copy = remote(
                hs.at[0, :, two], hs.at[1, :, two], hs_sem.at[0, b // 2], hs_sem.at[1, b // 2], partner
            )
            copy.start()
            hs_copies.append(copy)
    ocopies[0, 0].wait()
    ocopies[0, 1].wait()
    oacc[...] += jnp.dot(hs[0], ov[0, 0], preferred_element_type=F32)
    for copy in hs_copies:
        copy.wait_recv()
    out_ref[...] = (oacc[...] + jnp.dot(hs[1], ov[0, 1], preferred_element_type=F32)).astype(BF16)

    x_copy.wait_send()
    hc_copy.wait_send()
    for copy in hs_copies:
        copy.wait_send()

    @pl.when(sp < n - 1)
    def _():
        tail_copy.wait_send()

    def sent(j, c):
        end_copy(j).wait_send()
        return c

    lax.fori_loop(sp + 1, n, sent, 0)


def on_device(
    activations,
    norm_gain,
    state_proj,
    value_proj,
    post_gate_proj,
    pre_gate_proj,
    input_map,
    output_map,
    skip_gain,
    rotation,
    log_decay,
    initial_state,
    conv_taps,
    state_out,
    conv_out,
):
    n = lax.axis_size("sp")
    rows, half = activations.shape
    groups, state = rotation.shape
    chans = state_proj.shape[1]
    cwide = value_proj.shape[1]
    outs = state_out.shape[1]
    states = groups * state
    prow = states // LANES
    bdw = 2 * states // (chans // LANES)
    vmem = pl.BlockSpec(memory_space=pltpu.VMEM)
    hbm = pl.BlockSpec(memory_space=pl.ANY)
    dma = pltpu.SemaphoreType.DMA
    return pl.pallas_call(
        functools.partial(kernel, n),
        out_shape=jax.ShapeDtypeStruct((rows, outs), BF16),
        in_specs=[vmem, vmem, hbm, hbm, hbm, hbm] + [vmem] * 7 + [hbm, hbm],
        out_specs=vmem,
        scratch_shapes=[
            pltpu.VMEM((4, 2, half, chans), BF16),
            pltpu.VMEM((2, 2, chans, outs), BF16),
            pltpu.VMEM((rows, half), BF16),
            pltpu.VMEM((4, rows, chans), F32),
            pltpu.VMEM((rows, chans), BF16),
            pltpu.VMEM((chans, bdw), BF16),
            pltpu.VMEM((chans, bdw), BF16),
            pltpu.VMEM((rows, states), F32),
            pltpu.VMEM((rows * prow, LANES), F32),
            pltpu.VMEM((rows * 2 * prow, LANES), F32),
            pltpu.VMEM((3 * groups, LANES), F32),
            pltpu.VMEM((rows + 8, cwide), F32),
            pltpu.VMEM((3 * prow, LANES), F32),
            pltpu.VMEM((n, 3 * prow, LANES), F32),
            pltpu.VMEM((2, rows, chans), BF16),
            pltpu.VMEM((2, rows, cwide), BF16),
            pltpu.VMEM((rows, outs), F32),
            dma((4, 2)),
            dma((2, 2)),
            dma((2,)),
            dma((2,)),
            dma((2,)),
            dma((2, chans // (2 * LANES))),
            dma((n,)),
            dma((n,)),
        ],
        compiler_params=pltpu.CompilerParams(collective_id=0, has_side_effects=True),
    )(
        activations,
        norm_gain.reshape(1, -1),
        state_proj,
        value_proj,
        post_gate_proj,
        pre_gate_proj,
        input_map,
        jnp.swapaxes(output_map, 1, 2),
        skip_gain.reshape(1, -1),
        rotation,
        jnp.swapaxes(log_decay, 0, 1),
        initial_state,
        conv_taps,
        state_out,
        conv_out,
    )


def solution(mesh):
    return jax.shard_map(
        on_device,
        mesh=mesh,
        in_specs=(
            P("sp", "tp"),
            P(),
            P(None, "tp"),
            P(None, "tp"),
            P(None, "tp"),
            P(None, "tp"),
            P("tp", None, None),
            P("tp", None, None),
            P("tp"),
            P("tp", None),
            P("sp", "tp"),
            P(None, "tp", None),
            P(None, "tp"),
            P(None, "tp"),
            P(None, "tp"),
        ),
        out_specs=P("sp", "tp"),
        check_vma=False,
    )
```

time: 260 us -> 27.6 us (0.11)
  the two profiles are of different devices: /device:TPU:0 before, /device:TPU:17 now
where the time goes in v1:
time: 27.6 us; the launch traced here: 27.5 us
  Pallas kernels  25.8 us (93%)
  local copies, waits for them, and re-layouts  1.67 us (6%)
    pallas_call x1, Pallas kernels, on_device(): pl.pallas_call(functools.partial(kernel, n), out_shape=jax.ShapeDtypeStru...  25.8 us
    unnamed x1, local copies, waits for them, and re-layouts  1.67 us

profile of v1, /device:TPU:17, one launch (start us, length us, event | category | flops | bytes accessed | tf_op | source)
XLA Modules:
  0.0 27.5 jit_solution(2301779997611308313)
XLA Ops:
  0.0 25.8 %shard_map.145 = bf16[128,1024]{1,0:T(8,128)(2,1)} custom-call(bf16[128,1024]{1,0:T(8,128)(2,1)} %x_ref.1, f32[1,2048]{1,0:T(1,128)} %bitcast.6, bf16[2048,512]{1,0:T(8,128)(2,1)} %w0_hbm.1, bf16[2048,512]{1,0:T(8,128)(2,1)} %w1_hbm.1, bf16[2048,512]{1,0:T(8,128)(2,1)} %w2_hbm.1, bf16[2048,512]{1,0:T(8,128)(2,1)} %w3_hbm.1, bf16[32,16,128]{2,1,0:T(8,128)(2,1)} %imap_ref.1, ...), custom_call_target="tpu_custom_call" | custom-call | tf_op jit(solution)/shard_map/pallas_call | solution.py:388
  25.8 1.7 %copy.17 = bf16[128,1024]{1,0:T(8,128)(2,1)} copy(bf16[128,1024]{1,0:T(8,128)(2,1)} %shard_map.145) | data formatting | bytes 524288

commit v2 on v1

--- a/solution.py
+++ b/solution.py
@@ -50,12 +50,24 @@
 
 def kernel(
     n,
-    x_ref,
-    gain_ref,
+    x_hbm,
+    gain_hbm,
     w0_hbm,
     w1_hbm,
     w2_hbm,
     w3_hbm,
+    imap_hbm,
+    omap_hbm,
+    skip_hbm,
+    rot_hbm,
+    ld_hbm,
+    init_hbm,
+    taps_hbm,
+    so_hbm,
+    co_hbm,
+    out_ref,
+    x_ref,
+    gain_ref,
     imap_ref,
     omap_ref,
     skip_ref,
@@ -63,9 +75,6 @@
     ld_ref,
     init_ref,
     taps_ref,
-    so_hbm,
-    co_hbm,
-    out_ref,
     wv,
     ov,
     xr,
@@ -80,9 +89,12 @@
     pad,
     pay,
     ends,
+    tot,
+    tots,
     hs,
     hc,
     oacc,
+    in_sem,
     wsem,
     osem,
     x_sem,
@@ -91,6 +103,8 @@
     hs_sem,
     send_sem,
     recv_sem,
+    tsend_sem,
+    trecv_sem,
 ):
     sp, tp = lax.axis_index("sp"), lax.axis_index("tp")
     other = 1 - tp
@@ -103,6 +117,7 @@
     per_block = LANES // gch
     blocks = groups // per_block
     quads = prow // blocks
+    pitch = drv.shape[0] // rows
     bstates = quads * LANES
     cwide = taps_ref.shape[1]
     width = taps_ref.shape[0]
@@ -117,6 +132,22 @@
 
     pl.semaphore_signal(barrier, inc=1, device_id={"sp": sp, "tp": other}, device_id_type=MESH)
     lax.fori_loop(1, n, greet, 0)
+
+    small = []
+    for i, (src, dst) in enumerate((
+        (rot_hbm, rot_ref),
+        (init_hbm, init_ref),
+        (ld_hbm, ld_ref),
+        (imap_hbm, imap_ref),
+        (omap_hbm, omap_ref),
+        (x_hbm, x_ref),
+        (gain_hbm, gain_ref),
+        (skip_hbm, skip_ref),
+        (taps_hbm, taps_ref),
+    )):
+        copy = pltpu.make_async_copy(src, dst, in_sem.at[i])
+        copy.start()
+        small.append(copy)
 
     wcopies = {}
     for h, part in ((0, tp), (1, other)):
@@ -132,6 +163,9 @@
             copy = pltpu.make_async_copy(w.at[pl.ds(part * deep, deep), :], ov.at[i, h], osem.at[i, h])
             copy.start()
             ocopies[i, h] = copy
+
+    for copy in small:
+        copy.wait()
 
     lane = lax.broadcasted_iota(jnp.int32, (1, LANES), 1)
     for i, v in enumerate((rot_ref[...], init_ref[0], init_ref[1])):
@@ -164,6 +198,7 @@
 
     ld = ld_ref[...].T
     mags = split3(jnp.exp(ld))
+    whole_mags = split3(jnp.exp(jnp.sum(ld, axis=0, keepdims=True)))
     gains = split3(jnp.sqrt(minus_expm1(2.0 * ld)))[:2]
     for b in range(blocks):
         col = lax.broadcasted_iota(jnp.int32, (groups, bstates), 1) + b * bstates
@@ -182,6 +217,9 @@
         m = over(mags)
         for q in range(quads):
             mag[pl.ds(b * quads + q, rows, stride=prow), :] = m[:, q * LANES : (q + 1) * LANES]
+        m = over(whole_mags)
+        for q in range(quads):
+            tot[b * quads + q : b * quads + q + 1, :] = m[:, q * LANES : (q + 1) * LANES]
         wide_w[:, b * bstates : (b + 1) * bstates] = over(gains)
 
     pl.semaphore_wait(barrier, n)
@@ -194,6 +232,17 @@
 
     x_copy = remote(x_ref, xr, x_sem.at[0], x_sem.at[1], partner)
     x_copy.start()
+
+    def tot_copy(j):
+        return remote(
+            tot, tots.at[sp], tsend_sem.at[j], trecv_sem.at[sp], {"sp": j, "tp": tp}
+        )
+
+    def send_tot(j, c):
+        tot_copy(j).start()
+        return c
+
+    lax.fori_loop(sp + 1, n, send_tot, 0)
 
     own = x_ref[...].astype(F32)
     scaled = (own * gain_ref[:, pl.ds(pl.multiple_of(tp * half, LANES), half)]).astype(BF16)
@@ -224,30 +273,29 @@
         for q in range(quads):
             r = b * quads + q
             w = wide_w[:, r * LANES : (r + 1) * LANES]
-            drv[pl.ds(r, rows, stride=2 * prow), :] = blk[:, q * LANES : (q + 1) * LANES] * w
-            drv[pl.ds(prow + r, rows, stride=2 * prow), :] = (
+            drv[pl.ds(r, rows, stride=pitch), :] = blk[:, q * LANES : (q + 1) * LANES] * w
+            drv[pl.ds(prow + r, rows, stride=pitch), :] = (
                 blk[:, bstates + q * LANES : bstates + (q + 1) * LANES] * w
             )
 
     def advance(t, h):
         m = mag[pl.ds(pl.multiple_of(t * prow, prow), prow), :]
-        base = pl.multiple_of(t * 2 * prow, 2 * prow)
+        base = pl.multiple_of(t * pitch, 8)
         d_re = drv[pl.ds(base, prow), :]
         d_im = drv[pl.ds(base + prow, prow), :]
         f_re, f_im = m * cosv, m * sinv
         new_re = (f_re * h[0] + d_re) - f_im * h[1]
         new_im = (f_re * h[1] + d_im) + f_im * h[0]
-        return m, base, (new_re, new_im)
+        return base, (new_re, new_im)
 
     def first(t, c):
-        m, base, h = advance(t, c[:2])
-        return h[0], h[1], c[2] * m
+        base, h = advance(t, c)
+        return h
 
     zero = jnp.zeros((prow, LANES), F32)
-    e_re, e_im, e_mag = lax.fori_loop(0, rows, first, (zero, zero, zero + 1.0), unroll=8)
-    pay[pl.ds(0, prow), :] = e_re
-    pay[pl.ds(prow, prow), :] = e_im
-    pay[pl.ds(2 * prow, prow), :] = e_mag
+    e_re, e_im = lax.fori_loop(0, rows, first, (zero, zero), unroll=8)
+    pay[pl.ds(0, prow), :] = e_re.astype(BF16)
+    pay[pl.ds(prow, prow), :] = e_im.astype(BF16)
 
     def end_copy(j):
         return remote(
@@ -300,14 +348,17 @@
 
     def gather(k, h):
         remote(pay, ends.at[k], send_sem.at[k], recv_sem.at[k], {"sp": k, "tp": tp}).wait_recv()
-        k_mag = ends[k, pl.ds(2 * prow, prow), :]
+        remote(tot, tots.at[k], tsend_sem.at[k], trecv_sem.at[k], {"sp": k, "tp": tp}).wait_recv()
+        k_mag = tots[k]
         moved = cmul((whole[0] * k_mag, whole[1] * k_mag), h)
-        return moved[0] + ends[k, pl.ds(0, prow), :], moved[1] + ends[k, pl.ds(prow, prow), :]
+        k_re = ends[k, pl.ds(0, prow), :].astype(F32)
+        k_im = ends[k, pl.ds(prow, prow), :].astype(F32)
+        return moved[0] + k_re, moved[1] + k_im
 
     enter = lax.fori_loop(0, sp, gather, (paired(1), paired(2)))
 
     def second(t, c):
-        m, base, h = advance(t, c)
+        base, h = advance(t, c)
         drv[pl.ds(base, prow), :] = h[0]
         drv[pl.ds(base + prow, prow), :] = h[1]
         return h
@@ -320,7 +371,7 @@
         at = at + [prow + r for r in at]
         cols = slice(b * LANES, (b + 1) * LANES)
         st = jnp.concatenate(
-            [drv[pl.ds(r, rows, stride=2 * prow), :].astype(BF16) for r in at], axis=1
+            [drv[pl.ds(r, rows, stride=pitch), :].astype(BF16) for r in at], axis=1
         )
         read = lax.dot_general(
             st, bd_out[cols, :], (((1,), (1,)), ((), ())), preferred_element_type=F32
@@ -351,6 +402,7 @@
 
     def sent(j, c):
         end_copy(j).wait_send()
+        tot_copy(j).wait_send()
         return c
 
     lax.fori_loop(sp + 1, n, sent, 0)
@@ -387,10 +439,19 @@
     dma = pltpu.SemaphoreType.DMA
     return pl.pallas_call(
         functools.partial(kernel, n),
-        out_shape=jax.ShapeDtypeStruct((rows, outs), BF16),
-        in_specs=[vmem, vmem, hbm, hbm, hbm, hbm] + [vmem] * 7 + [hbm, hbm],
+        out_shape=pltpu.VMEM((rows, outs), BF16),
+        in_specs=[hbm] * 15,
         out_specs=vmem,
         scratch_shapes=[
+            pltpu.VMEM((rows, half), BF16),
+            pltpu.VMEM((1, 2 * half), F32),
+            pltpu.VMEM(input_map.shape, BF16),
+            pltpu.VMEM((groups, output_map.shape[2], output_map.shape[1]), F32),
+            pltpu.VMEM((1, chans), F32),
+            pltpu.VMEM((groups, state), F32),
+            pltpu.VMEM((groups, rows), F32),
+            pltpu.VMEM(initial_state.shape, F32),
+            pltpu.VMEM(conv_taps.shape, BF16),
             pltpu.VMEM((4, 2, half, chans), BF16),
             pltpu.VMEM((2, 2, chans, outs), BF16),
             pltpu.VMEM((rows, half), BF16),
@@ -400,20 +461,25 @@
             pltpu.VMEM((chans, bdw), BF16),
             pltpu.VMEM((rows, states), F32),
             pltpu.VMEM((rows * prow, LANES), F32),
-            pltpu.VMEM((rows * 2 * prow, LANES), F32),
+            pltpu.VMEM((rows * (2 * prow + 8), LANES), F32),
             pltpu.VMEM((3 * groups, LANES), F32),
             pltpu.VMEM((rows + 8, cwide), F32),
-            pltpu.VMEM((3 * prow, LANES), F32),
-            pltpu.VMEM((n, 3 * prow, LANES), F32),
+            pltpu.VMEM((2 * prow, LANES), BF16),
+            pltpu.VMEM((n, 2 * prow, LANES), BF16),
+            pltpu.VMEM((prow, LANES), F32),
+            pltpu.VMEM((n, prow, LANES), F32),
             pltpu.VMEM((2, rows, chans), BF16),
             pltpu.VMEM((2, rows, cwide), BF16),
             pltpu.VMEM((rows, outs), F32),
+            dma((9,)),
             dma((4, 2)),
             dma((2, 2)),
             dma((2,)),
             dma((2,)),
             dma((2,)),
             dma((2, chans // (2 * LANES))),
+            dma((n,)),
+            dma((n,)),
             dma((n,)),
             dma((n,)),
         ],

time: 27.6 us -> 21 us (0.76)
  Pallas kernels: 25.8 us -> 20 us
  local copies, waits for them, and re-layouts: 1.67 us -> 0.71 us
    pallas_call x1, Pallas kernels: 25.8 us -> 20 us  [on_device(): pl.pallas_call(functools.partial(kernel, n), out_shape=pltpu.VMEM((rows,...]
    unnamed x1, local copies, waits for them, and re-layouts: 1.67 us -> 0.71 us
where the time goes in v2:
time: 21 us; the launch traced here: 20.7 us
  Pallas kernels  20 us (95%)
  local copies, waits for them, and re-layouts  0.71 us (3%)
    pallas_call x1, Pallas kernels, on_device(): pl.pallas_call(functools.partial(kernel, n), out_shape=pltpu.VMEM((rows,...  20 us
    unnamed x1, local copies, waits for them, and re-layouts  0.71 us

profile of v2, /device:TPU:17, one launch (start us, length us, event | category | flops | bytes accessed | tf_op | source)
XLA Modules:
  0.0 20.7 jit_solution(13469114048519505066)
XLA Ops:
  0.0 20.0 %shard_map.145 = bf16[128,1024]{1,0:T(8,128)(2,1)S(1)} custom-call(bf16[128,1024]{1,0:T(8,128)(2,1)} %x_hbm.1, f32[1,2048]{1,0:T(1,128)} %bitcast.6, bf16[2048,512]{1,0:T(8,128)(2,1)} %w0_hbm.1, bf16[2048,512]{1,0:T(8,128)(2,1)} %w1_hbm.1, bf16[2048,512]{1,0:T(8,128)(2,1)} %w2_hbm.1, bf16[2048,512]{1,0:T(8,128)(2,1)} %w3_hbm.1, ...), custom_call_target="tpu_custom_call" | custom-call | tf_op jit(solution)/shard_map/pallas_call | solution.py:440
  20.0 0.7 %copy.17 = bf16[128,1024]{1,0:T(8,128)(2,1)} copy(bf16[128,1024]{1,0:T(8,128)(2,1)S(1)} %shard_map.145) | data formatting | bytes 524288

commit v3 on v2

--- a/solution.py
+++ b/solution.py
@@ -133,30 +133,35 @@
     pl.semaphore_signal(barrier, inc=1, device_id={"sp": sp, "tp": other}, device_id_type=MESH)
     lax.fori_loop(1, n, greet, 0)
 
-    small = []
-    for i, (src, dst) in enumerate((
-        (rot_hbm, rot_ref),
-        (init_hbm, init_ref),
-        (ld_hbm, ld_ref),
-        (imap_hbm, imap_ref),
-        (omap_hbm, omap_ref),
-        (x_hbm, x_ref),
-        (gain_hbm, gain_ref),
-        (skip_hbm, skip_ref),
-        (taps_hbm, taps_ref),
-    )):
-        copy = pltpu.make_async_copy(src, dst, in_sem.at[i])
-        copy.start()
-        small.append(copy)
+    in_copies = {}
+    def fetch(i, src, dst):
+        in_copies[i] = pltpu.make_async_copy(src, dst, in_sem.at[i])
+        in_copies[i].start()
 
     wcopies = {}
-    for h, part in ((0, tp), (1, other)):
-        for i, w in enumerate((w0_hbm, w1_hbm, w2_hbm, w3_hbm)):
-            copy = pltpu.make_async_copy(
-                w.at[pl.ds(part * half, half), :], wv.at[i, h], wsem.at[i, h]
-            )
-            copy.start()
-            wcopies[i, h] = copy
+
+    def fetch_weight(i, h):
+        w = (w0_hbm, w1_hbm, w2_hbm, w3_hbm)[i]
+        part = (tp, other)[h]
+        wcopies[i, h] = pltpu.make_async_copy(
+            w.at[pl.ds(part * half, half), :], wv.at[i, h], wsem.at[i, h]
+        )
+        wcopies[i, h].start()
+
+    fetch(0, x_hbm, x_ref)
+    fetch(1, gain_hbm, gain_ref)
+    fetch(2, rot_hbm, rot_ref)
+    fetch(3, init_hbm, init_ref)
+    fetch(4, ld_hbm, ld_ref)
+    fetch(5, imap_hbm, imap_ref)
+    fetch_weight(0, 0)
+    fetch_weight(0, 1)
+    fetch(6, omap_hbm, omap_ref)
+    fetch(7, skip_hbm, skip_ref)
+    fetch(8, taps_hbm, taps_ref)
+    for i in (1, 3, 2):
+        fetch_weight(i, 0)
+        fetch_weight(i, 1)
     ocopies = {}
     for i, w, deep in ((1, co_hbm, cwide), (0, so_hbm, chans)):
         for h, part in ((0, tp), (1, other)):
@@ -164,8 +169,20 @@
             copy.start()
             ocopies[i, h] = copy
 
-    for copy in small:
-        copy.wait()
+    pl.semaphore_wait(barrier, n)
+    partner = {"sp": sp, "tp": other}
+
+    def remote(src, dst, s, r, dev):
+        return pltpu.make_async_remote_copy(
+            src_ref=src, dst_ref=dst, send_sem=s, recv_sem=r, device_id=dev, device_id_type=MESH
+        )
+
+    in_copies[0].wait()
+    x_copy = remote(x_ref, xr, x_sem.at[0], x_sem.at[1], partner)
+    x_copy.start()
+
+    for i in range(2, 6):
+        in_copies[i].wait()
 
     lane = lax.broadcasted_iota(jnp.int32, (1, LANES), 1)
     for i, v in enumerate((rot_ref[...], init_ref[0], init_ref[1])):
@@ -180,7 +197,7 @@
     cosv, sinv = jnp.cos(theta), jnp.sin(theta)
     whole = cpow((cosv, sinv), rows)
 
-    for src, dst in ((imap_ref, bd_in), (omap_ref, bd_out)):
+    def spread_map(src, dst):
         dst[...] = jnp.zeros_like(dst)
         for b in range(blocks):
             for q in range(quads):
@@ -196,6 +213,8 @@
                 dst[at, q * LANES : (q + 1) * LANES] = re.astype(BF16)
                 dst[at, bstates + q * LANES : bstates + (q + 1) * LANES] = im.astype(BF16)
 
+    spread_map(imap_ref, bd_in)
+
     ld = ld_ref[...].T
     mags = split3(jnp.exp(ld))
     whole_mags = split3(jnp.exp(jnp.sum(ld, axis=0, keepdims=True)))
@@ -222,17 +241,6 @@
             tot[b * quads + q : b * quads + q + 1, :] = m[:, q * LANES : (q + 1) * LANES]
         wide_w[:, b * bstates : (b + 1) * bstates] = over(gains)
 
-    pl.semaphore_wait(barrier, n)
-    partner = {"sp": sp, "tp": other}
-
-    def remote(src, dst, s, r, dev):
-        return pltpu.make_async_remote_copy(
-            src_ref=src, dst_ref=dst, send_sem=s, recv_sem=r, device_id=dev, device_id_type=MESH
-        )
-
-    x_copy = remote(x_ref, xr, x_sem.at[0], x_sem.at[1], partner)
-    x_copy.start()
-
     def tot_copy(j):
         return remote(
             tot, tots.at[sp], tsend_sem.at[j], trecv_sem.at[sp], {"sp": j, "tp": tp}
@@ -244,12 +252,13 @@
 
     lax.fori_loop(sp + 1, n, send_tot, 0)
 
+    in_copies[1].wait()
     own = x_ref[...].astype(F32)
     scaled = (own * gain_ref[:, pl.ds(pl.multiple_of(tp * half, LANES), half)]).astype(BF16)
     squares = jnp.sum(own * own, axis=1, keepdims=True)
-    for i in range(4):
-        wcopies[i, 0].wait()
-        acc[i] = jnp.dot(scaled, wv[i, 0], preferred_element_type=F32)
+    wcopies[0, 0].wait()
+    partial = jnp.dot(scaled, wv[0, 0], preferred_element_type=F32)
+    acc[0] = scaled
 
     x_copy.wait_recv()
     far = xr[...].astype(F32)
@@ -257,12 +266,10 @@
     squares = squares + jnp.sum(far * far, axis=1, keepdims=True)
     scale = lax.rsqrt(squares / (2 * half) + EPS)
 
-    def project(i):
-        wcopies[i, 1].wait()
-        total = acc[i] + jnp.dot(scaled_far, wv[i, 1], preferred_element_type=F32)
-        return (total * scale).astype(BF16)
-
-    drive_in = project(0)
+    acc[1] = scaled_far
+    wcopies[0, 1].wait()
+    total = partial + jnp.dot(scaled_far, wv[0, 1], preferred_element_type=F32)
+    drive_in = (total * scale).astype(BF16)
     din[...] = drive_in
     for b in range(blocks):
         blk = jnp.dot(
@@ -307,6 +314,13 @@
         return c
 
     lax.fori_loop(sp + 1, n, send_end, 0)
+
+    def project(i):
+        wcopies[i, 0].wait()
+        wcopies[i, 1].wait()
+        total = jnp.dot(acc[0], wv[i, 0], preferred_element_type=F32)
+        total = total + jnp.dot(acc[1], wv[i, 1], preferred_element_type=F32)
+        return (total * scale).astype(BF16)
 
     value = project(1)
     pre_gate = project(3)
@@ -324,27 +338,11 @@
     def _():
         tail_copy.start()
 
-    post_gate = project(2).astype(F32)
-
-    @pl.when(sp == 0)
-    def _():
-        pad[pl.ds(0, 8), :] = jnp.zeros((8, cwide), F32)
-
-    @pl.when(sp > 0)
-    def _():
-        tail_copy.wait_recv()
-
-    conv = jnp.zeros((rows, cwide), F32)
-    for k in range(width):
-        conv = conv + pad[pl.ds(8 + k - (width - 1), rows), :] * taps_ref[k : k + 1, :].astype(F32)
-    hc[0] = (post_gate * conv).astype(BF16)
-    hc_copy = remote(hc.at[0], hc.at[1], hc_sem.at[0], hc_sem.at[1], partner)
-    hc_copy.start()
-    ocopies[1, 0].wait()
-    ocopies[1, 1].wait()
-    oacc[...] = jnp.dot(hc[0], ov[1, 0], preferred_element_type=F32)
-    hc_copy.wait_recv()
-    oacc[...] += jnp.dot(hc[1], ov[1, 1], preferred_element_type=F32)
+    hc[0] = project(2)
+
+    for i in (6, 7):
+        in_copies[i].wait()
+    spread_map(omap_ref, bd_out)
 
     def gather(k, h):
         remote(pay, ends.at[k], send_sem.at[k], recv_sem.at[k], {"sp": k, "tp": tp}).wait_recv()
@@ -365,6 +363,22 @@
 
     lax.fori_loop(0, rows, second, enter, unroll=8)
 
+    @pl.when(sp == 0)
+    def _():
+        pad[pl.ds(0, 8), :] = jnp.zeros((8, cwide), F32)
+
+    in_copies[8].wait()
+
+    @pl.when(sp > 0)
+    def _():
+        tail_copy.wait_recv()
+
+    conv = jnp.zeros((rows, cwide), F32)
+    for k in range(width):
+        conv = conv + pad[pl.ds(8 + k - (width - 1), rows), :] * taps_ref[k : k + 1, :].astype(F32)
+    hc[0] = (hc[0].astype(F32) * conv).astype(BF16)
+    hc_copy = remote(hc.at[0], hc.at[1], hc_sem.at[0], hc_sem.at[1], partner)
+    hc_copy.start()
     hs_copies = []
     for b in range(blocks):
         at = [b * quads + q for q in range(quads)]
@@ -384,9 +398,13 @@
             )
             copy.start()
             hs_copies.append(copy)
-    ocopies[0, 0].wait()
-    ocopies[0, 1].wait()
+    for i in (0, 1):
+        for h in (0, 1):
+            ocopies[i, h].wait()
+    oacc[...] = jnp.dot(hc[0], ov[1, 0], preferred_element_type=F32)
     oacc[...] += jnp.dot(hs[0], ov[0, 0], preferred_element_type=F32)
+    hc_copy.wait_recv()
+    oacc[...] += jnp.dot(hc[1], ov[1, 1], preferred_element_type=F32)
     for copy in hs_copies:
         copy.wait_recv()
     out_ref[...] = (oacc[...] + jnp.dot(hs[1], ov[0, 1], preferred_element_type=F32)).astype(BF16)
@@ -455,7 +473,7 @@
             pltpu.VMEM((4, 2, half, chans), BF16),
             pltpu.VMEM((2, 2, chans, outs), BF16),
             pltpu.VMEM((rows, half), BF16),
-            pltpu.VMEM((4, rows, chans), F32),
+            pltpu.VMEM((2, rows, half), BF16),
             pltpu.VMEM((rows, chans), BF16),
             pltpu.VMEM((chans, bdw), BF16),
             pltpu.VMEM((chans, bdw), BF16),

time: 21 us -> 17.3 us (0.82)
  Pallas kernels: 20 us -> 16.4 us
    pallas_call x1, Pallas kernels: 20 us -> 16.4 us  [on_device(): pl.pallas_call(functools.partial(kernel, n), out_shape=pltpu.VMEM((rows,...]
where the time goes in v3:
time: 17.3 us; the launch traced here: 17.1 us
  Pallas kernels  16.4 us (95%)
  local copies, waits for them, and re-layouts  0.71 us (4%)
    pallas_call x1, Pallas kernels, on_device(): pl.pallas_call(functools.partial(kernel, n), out_shape=pltpu.VMEM((rows,...  16.4 us
    unnamed x1, local copies, waits for them, and re-layouts  0.71 us

profile of v3, /device:TPU:17, one launch (start us, length us, event | category | flops | bytes accessed | tf_op | source)
XLA Modules:
  0.0 17.1 jit_solution(7419787779171471081)
XLA Ops:
  0.0 16.4 %shard_map.145 = bf16[128,1024]{1,0:T(8,128)(2,1)S(1)} custom-call(bf16[128,1024]{1,0:T(8,128)(2,1)} %x_hbm.1, f32[1,2048]{1,0:T(1,128)} %bitcast.6, bf16[2048,512]{1,0:T(8,128)(2,1)} %w0_hbm.1, bf16[2048,512]{1,0:T(8,128)(2,1)} %w1_hbm.1, bf16[2048,512]{1,0:T(8,128)(2,1)} %w2_hbm.1, bf16[2048,512]{1,0:T(8,128)(2,1)} %w3_hbm.1, ...), custom_call_target="tpu_custom_call" | custom-call | tf_op jit(solution)/shard_map/pallas_call | solution.py:458
  16.4 0.7 %copy.17 = bf16[128,1024]{1,0:T(8,128)(2,1)} copy(bf16[128,1024]{1,0:T(8,128)(2,1)S(1)} %shard_map.145) | data formatting | bytes 524288
